TPU v7x, 256 devices: a whole 4x4x8 slice. The times are simulated.
256 devices in a mesh: sp: 32 (over z, x), tp: 8 (over y, core).
Axes of the slice: x: 4, y: 4, z: 8, core: 2. Of those that a mesh axis runs over, the one named last changes fastest.
Arguments:
- latents: bfloat16 [16384, 2048], P(('sp', 'tp')), may hold values from -6 to 6
- context: bfloat16 [512, 2048], P('sp'), may hold values from -6 to 6
- cond: float32 [2048], P('sp'), may hold values from -6 to 6
- ctx_cond: float32 [2048], P('sp'), may hold values from -6 to 6
- mod_weight: float32 [2048, 6144], P('sp', 'tp'), may hold values from -0.125 to 0.125
- query_weight: bfloat16 [2048, 2048], P(None, 'tp'), may hold values from -1 to 1, as said below
- key_matrix: bfloat16 [2048, 1024], P(None, 'tp'), may hold values from -1 to 1, as said below
- value_matrix: bfloat16 [2048, 1024], P(None, 'tp'), may hold values from -0.125 to 0.125
- out_weight: bfloat16 [2048, 2048], P('tp'), may hold values from -0.125 to 0.125
- query_gain: float32 [128], replicated, may hold values from 0.7 to 7
- key_gain: float32 [128], replicated, may hold values from 0.7 to 7
Outputs:
- updated: bfloat16 [16384, 2048], P(('sp', 'tp'))
Inputs may be any that keep to these rules, and one draw needn't show every extreme that they name: `query_weight`: entries of order 2048 to the power -1/2. `key_matrix`: entries of order 2048 to the power -1/2.
All inputs are finite; a program needn't handle non-finite values.
Results may differ from a plain program's by a relative error of at most 0.0085.
The roundings to bfloat16 on the way count: a program that leaves them out, or rounds other values in their place, can miss the bound.
Values may be sent and summed in bfloat16 or wider, within the bound.
No kernel may reach another device: no remote copies, remote signals or barrier semaphores. Data moves between devices by JAX's collectives and lax.ppermute only.
A program may use at most 128 MiB of HBM per device.

v0:
```python
import math
import jax
import jax.numpy as jnp
from jax import lax
from jax.sharding import Mesh
from jax.sharding import PartitionSpec as P

GRID_W = 64
SP = ("sp_0", "sp_1")
SP_TP = ("sp_0", "sp_1", "tp")
NORM_EPS = 1e-06
ROPE_BASE = 10000.0


def over_axes(value, axes):
    for axis in axes:
        value = lax.psum(value, axis)
    return value


def side_by_side(arrays, axis, dim, along):
    both = jnp.concatenate(arrays, axis=along)
    filled, at, done = (lax.all_gather(both, axis, axis=dim, tiled=True), 0, [])
    for a in arrays:
        done.append(lax.slice_in_dim(filled, at, at + a.shape[along], axis=along))
        at += a.shape[along]
    return tuple(done)


def normalize(latent_value_rows):
    return latent_value_rows * lax.rsqrt(
        jnp.mean(latent_value_rows * latent_value_rows, axis=-1, keepdims=True) + NORM_EPS
    )


def rotate(latent_value_rows, positions):
    quarter = latent_value_rows.shape[-1] // 2
    inv_freq = ROPE_BASE ** (-jnp.arange(quarter, dtype=jnp.float32) / quarter)
    angles = positions.astype(jnp.float32)[:, None] * inv_freq[None, :]
    cos_table = jnp.cos(angles)[:, None, :]
    sin_table = jnp.sin(angles)[:, None, :]
    first, second = (latent_value_rows[..., :quarter], latent_value_rows[..., quarter:])
    return jnp.concatenate(
        [first * cos_table - second * sin_table, second * cos_table + first * sin_table], axis=-1
    )


def axial(latent_value_rows, positions):
    half_dim = latent_value_rows.shape[-1] // 2
    return jnp.concatenate(
        [
            rotate(latent_value_rows[..., :half_dim], positions // GRID_W),
            rotate(latent_value_rows[..., half_dim:], positions % GRID_W),
        ],
        axis=-1,
    )


def modulate(latent_value_rows, mod_row):
    model_width = latent_value_rows.shape[-1]
    shift_vec = mod_row[:model_width]
    scale_vec = mod_row[model_width : 2 * model_width]
    return (
        normalize(latent_value_rows.astype(jnp.float32)) * (1.0 + scale_vec) + shift_vec
    ).astype(jnp.bfloat16)


def body(
    latents,
    context,
    cond,
    ctx_cond,
    mod_weight,
    query_weight,
    key_matrix,
    value_matrix,
    out_weight,
    query_gain,
    key_gain,
):
    model_width = latents.shape[1]
    head_dim = query_gain.shape[0]
    sp_count = lax.axis_size(SP)
    partials = jnp.dot(
        jax.nn.silu(jnp.stack([cond, ctx_cond])), mod_weight, precision=lax.Precision.HIGHEST
    )
    summed = over_axes(partials, SP)
    modulation = lax.all_gather(summed, "tp", axis=1, tiled=True)
    gate_vec = modulation[0, 2 * model_width :]
    normalised_rows = modulate(latents, modulation[0])
    prefix_normalised = modulate(context, modulation[1])
    query_cols = query_weight.shape[1]
    key_cols = key_matrix.shape[1]
    piece = lax.all_gather(normalised_rows, "tp", axis=0, tiled=True)
    projected = jnp.concatenate(
        [
            jnp.dot(piece, query_weight, preferred_element_type=jnp.float32),
            jnp.dot(piece, key_matrix, preferred_element_type=jnp.float32),
            jnp.dot(piece, value_matrix, preferred_element_type=jnp.float32),
        ],
        axis=1,
    )
    row_count = projected.shape[0]
    positions = lax.axis_index(SP) * row_count + jnp.arange(row_count, dtype=jnp.int32)
    query_heads = projected[:, :query_cols].reshape(row_count, -1, head_dim)
    query_heads = axial(normalize(query_heads) * query_gain, positions).astype(jnp.bfloat16)
    key_heads = projected[:, query_cols : query_cols + key_cols].reshape(row_count, -1, head_dim)
    key_heads = axial(normalize(key_heads) * key_gain, positions).astype(jnp.bfloat16)
    value_heads = (
        projected[:, query_cols + key_cols :].reshape(row_count, -1, head_dim).astype(jnp.bfloat16)
    )
    key_part = jnp.dot(prefix_normalised, key_matrix, preferred_element_type=jnp.float32).reshape(
        prefix_normalised.shape[0], -1, head_dim
    )
    value_part = jnp.dot(
        prefix_normalised, value_matrix, preferred_element_type=jnp.float32
    ).reshape(prefix_normalised.shape[0], -1, head_dim)
    local_keys = (normalize(key_part) * key_gain).astype(jnp.bfloat16)
    local_values = value_part.astype(jnp.bfloat16)
    prefix_keys, prefix_values = side_by_side((local_keys, local_values), SP, 0, 1)
    kv_local = key_heads.shape[1]
    group_size = query_heads.shape[1] // kv_local
    grouped = query_heads.reshape(row_count, kv_local, group_size, head_dim).transpose(1, 2, 0, 3)
    grouped = grouped.reshape(kv_local, group_size * row_count, head_dim)
    inv_root = head_dim ** (-0.5)
    lift = math.log(sp_count * row_count / (2.0 * prefix_keys.shape[0]))
    ctx_scores = (
        jnp.einsum("hqd,khd->hqk", grouped, prefix_keys, preferred_element_type=jnp.float32)
        * inv_root
        + lift
    )
    top_init = jnp.max(ctx_scores, axis=-1)
    ctx_weights = jnp.exp(ctx_scores - top_init[..., None])
    initial = (
        top_init,
        jnp.sum(ctx_weights, axis=-1),
        jnp.einsum(
            "hqk,khd->hqd",
            ctx_weights.astype(jnp.bfloat16),
            prefix_values,
            preferred_element_type=jnp.float32,
        ),
    )

    def update(state_now, key_block, value_block):
        top_old, total_old, acc_old = state_now
        scores = (
            jnp.einsum("hqd,khd->hqk", grouped, key_block, preferred_element_type=jnp.float32)
            * inv_root
        )
        top_new = jnp.maximum(top_old, jnp.max(scores, axis=-1))
        factor = jnp.exp(top_old - top_new)
        weights_now = jnp.exp(scores - top_new[..., None])
        acc_new = acc_old * factor[..., None] + jnp.einsum(
            "hqk,khd->hqd",
            weights_now.astype(jnp.bfloat16),
            value_block,
            preferred_element_type=jnp.float32,
        )
        return (top_new, total_old * factor + jnp.sum(weights_now, axis=-1), acc_new)

    key_piece, value_piece = side_by_side((key_heads, value_heads), SP, 0, 1)
    key_count = key_piece.shape[0]
    rows_per_block = math.gcd(key_count, 2048)
    block_count = key_count // rows_per_block
    key_blocks = key_piece.reshape(block_count, rows_per_block, kv_local, head_dim)
    value_blocks = value_piece.reshape(block_count, rows_per_block, kv_local, head_dim)

    def one_step(state_in, blocks_in):
        return (update(state_in, blocks_in[0], blocks_in[1]), None)

    state_out, _ = lax.scan(one_step, initial, (key_blocks, value_blocks))
    top_fin, total_fin, acc_fin = state_out
    attended = (acc_fin / total_fin[..., None]).astype(jnp.bfloat16)
    attended = (
        attended.reshape(kv_local, group_size, row_count, head_dim)
        .transpose(2, 0, 1, 3)
        .reshape(row_count, -1)
    )
    exchanged = lax.all_to_all(attended, "tp", split_axis=0, concat_axis=1, tiled=True)
    mixed_rows = jnp.dot(
        exchanged,
        lax.all_gather(out_weight, "tp", axis=0, tiled=True),
        preferred_element_type=jnp.float32,
    )
    return (latents.astype(jnp.float32) + gate_vec * normalize(mixed_rows)).astype(jnp.bfloat16)


def solution(mesh):
    torus = Mesh(mesh.devices.reshape(8, 4, mesh.shape["tp"]), ("sp_0", "sp_1", "tp"))
    placed = (
        P(SP_TP, None),
        P(SP, None),
        P(SP),
        P(SP),
        P(SP, "tp"),
        P(None, "tp"),
        P(None, "tp"),
        P(None, "tp"),
        P("tp", None),
        P(),
        P(),
    )
    return jax.shard_map(
        body, mesh=torus, in_specs=placed, out_specs=P(SP_TP, None), check_vma=False
    )
```

profile of v0, /device:TPU:1, one launch (start us, length us, event | category | flops | bytes accessed | tf_op | source)
XLA Modules:
  0.0 285.0 jit_solution(6609689054624795851)
XLA Ops:
  7.8 17.5 %psum.14 = f32[2,768]{1,0:T(2,128)S(1)} all-reduce(f32[2,768]{1,0:T(2,128)S(1)} %fusion.67), channel_id=1, replica_groups=mesh['sp_0'=8,'sp_1'=4,'tp'=8] {'sp_0'}, use_global_device_ids=true, to_apply=%region_0.1 | all-reduce | flops 1536 | bytes 12288 | tf_op jit(solution)/shard_map/psum | solution.py:17
  25.3 8.6 %psum.15 = f32[2,768]{1,0:T(2,128)S(1)} all-reduce(f32[2,768]{1,0:T(2,128)S(1)} %psum.14), channel_id=1, replica_groups=mesh['sp_0'=8,'sp_1'=4,'tp'=8] {'sp_1'}, use_global_device_ids=true, to_apply=%region_1.2 | all-reduce | flops 1536 | bytes 12288 | tf_op jit(solution)/shard_map/psum | solution.py:17
  33.9 19.5 %all_gather.15 = f32[2,6144]{1,0:T(2,128)S(1)} all-gather(f32[2,768]{1,0:T(2,128)S(1)} %psum.15), channel_id=1, replica_groups=mesh['sp_0'=8,'sp_1'=4,'tp'=8] {'tp'}, dimensions={1}, use_global_device_ids=true | all-gather | bytes 55296 | tf_op jit(solution)/shard_map/all_gather | solution.py:88
  56.5 23.1 %all-gather.4.cloned.1.call-done = bf16[512,2048]{1,0:T(8,128)(2,1)} async-done(((bf16[64,2048]{1,0:T(8,128)(2,1)}), bf16[512,2048]{1,0:T(8,128)(2,1)}) %all-gather.4.cloned.1.call-update) | async-done | bytes 2097168 | tf_op jit(solution)/shard_map/all_gather | solution.py:94
  79.5 2.5 multiply_reduce_fusion.3
  82.7 2.5 fusion.22
  86.8 3.0 %multiply_cosine_fusion.1 = (f32[512,32]{1,0:T(8,128)S(1)}, f32[512,32]{1,0:T(8,128)}, f32[512,32]{1,0:T(8,128)}, f32[512,32]{1,0:T(8,128)}) fusion(f32[32]{0:T(128)S(1)} %multiply_power_fusion, f32[512]{0:T(512)S(1)} %get-tuple-element.112, f32[512]{0:T(512)S(1)} %get-tuple-element.113), kind=kLoop, calls=%fused_computation.50 | loop fusion | flops 32768 | bytes 266368 | tf_op jit(solution)/shard_map/cos | solution.py:40
  92.6 40.4 %all_gather.17 = bf16[512,2,128]{2,0,1:T(8,128)(2,1)} all-gather(bf16[16,2,128]{2,0,1:T(8,128)(2,1)S(1)} %pad_maximum_fusion.2), channel_id=1, replica_groups=mesh['sp_0'=8,'sp_1'=4,'tp'=8] {'sp_0','sp_1'}, dimensions={0}, use_global_device_ids=true | all-gather | bytes 270336 | tf_op jit(solution)/shard_map/all_gather | solution.py:23
  139.6 46.4 %all-gather.6.cloned.1.call-done = bf16[16384,2,128]{0,2,1:T(8,128)(2,1)} async-done(((bf16[512,2,128]{0,2,1:T(8,128)(2,1)}), bf16[16384,2,128]{0,2,1:T(8,128)(2,1)}) %all-gather.6.cloned.1.call-update) | async-done | bytes 8388624 | tf_op jit(solution)/shard_map/all_gather | solution.py:23
  186.1 5.8 %fusion.76 = (bf16[16384,1,128]{0,2,1:T(8,128)(2,1)}, bf16[16384,1,128]{0,2,1:T(8,128)(2,1)}) fusion(bf16[16384,2,128]{0,2,1:T(8,128)(2,1)} %all-gather.6.cloned.1.call-done), kind=kLoop, calls=%fused_computation.126 | loop fusion | bytes 16777216 | tf_op jit(solution)/shard_map/slice | solution.py:25
  191.9 6.3 %copy.23 = bf16[16384,1,128]{2,0,1:T(8,128)(2,1)} copy(bf16[16384,1,128]{0,2,1:T(8,128)(2,1)} %get-tuple-element.78) | data formatting | bytes 8388608 | tf_op jit(solution)/shard_map/while | solution.py:172
  198.2 6.5 %copy.24 = bf16[16384,1,128]{2,0,1:T(8,128)(2,1)} copy(bf16[16384,1,128]{0,2,1:T(8,128)(2,1)} %get-tuple-element.77) | data formatting | bytes 8388608 | tf_op jit(solution)/shard_map/while | solution.py:172
  204.7 52.6 %while.14 = (s32[]{:T(128)}, f32[1,1024]{1,0:T(1,128)S(1)}, f32[1,1024]{1,0:T(1,128)S(1)}, f32[1,1024,128]{2,1,0:T(8,128)S(1)}, bf16[8,2048,1,128]{3,1,2,0:T(8,1...) while((s32[]{:T(128)}, f32[1,1024]{1,0:T(1,128)S(1)}, ...), condition=%wide.region_12.13_spmd, body=%wide.region_9.12_spmd.sunk | while | flops 1090783232 | bytes 27590756 | solution.py:172
  204.7 2.3 multiply_reduce_fusion.6
  208.5 2.8 fusion.97
  215.1 2.8 fusion.97
  221.6 2.8 fusion.97
  228.2 2.8 fusion.97
  234.8 2.8 fusion.97
  241.4 2.8 fusion.97
  247.9 2.8 fusion.97
  254.5 2.8 fusion.97
  258.0 14.5 %all_to_all.19 = bf16[8,64,256]{2,1,0:T(8,128)(2,1)S(1)} all-to-all(bf16[8,64,256]{2,1,0:T(8,128)(2,1)S(1)} %all_to_all.14), channel_id=1, replica_groups=mesh['sp_0'=8,'sp_1'=4,'tp'=8] {'tp'}, dimensions={0} | all-to-all | bytes 524288 | tf_op jit(solution)/shard_map/all_to_all | solution.py:180
  272.5 5.1 %multiply_reduce_fusion.1 = (f32[64]{0:T(128)S(1)}, f32[64,2048]{1,0:T(8,128)S(1)}) fusion(bf16[64,2048]{1,0:T(8,128)(2,1)S(1)} %bitcast.110, bf16[2048,2048]{1,0:T(8,128)(2,1)} %all-gather.8.cloned.1.call-done), kind=kOutput, calls=%fused_computation.39 | convolution fusion | flops 537132992 | bytes 9175296 | tf_op jit(solution)/shard_map/dot_general | solution.py:181
  (93 shorter events, 45.2 us)
Async XLA Ops:
  6.5 126.6 %copy-start = (bf16[2048,256]{1,0:T(8,128)(2,1)S(1)}, bf16[2048,256]{1,0:T(8,128)(2,1)}, u32[]{:S(2)}) copy-start(bf16[2048,256]{1,0:T(8,128)(2,1)} %param.18) | copy-start | bytes 3145732
  6.5 75.5 %copy-start.5 = (f32[128]{0:T(128)S(1)}, f32[128]{0:T(128)}, u32[]{:S(2)}) copy-start(f32[128]{0:T(128)} %param.23) | copy-start | bytes 1540
  6.5 73.0 %all-gather.4.cloned.1.call-start = ((), (), s32[]{:S(2)}) async-start(), calls=%async_computation.1 | async-start | bytes 2359296 | tf_op jit(solution)/shard_map/all_gather | solution.py:94
  56.4 129.7 %all-gather.6.cloned.1.call-start = ((), (), s32[]{:S(2)}) async-start(), calls=%async_computation.2 | async-start | bytes 8650752 | tf_op jit(solution)/shard_map/all_gather | solution.py:23
  56.4 33.3 %copy-start.4 = (bf16[16,2048]{1,0:T(8,128)(2,1)S(1)}, bf16[16,2048]{1,0:T(8,128)(2,1)}, u32[]{:S(2)}) copy-start(bf16[16,2048]{1,0:T(8,128)(2,1)} %param.14) | copy-start | bytes 196612
  82.1 51.0 %copy-start.1 = (bf16[512,2048]{1,0:T(8,128)(2,1)S(1)}, bf16[512,2048]{1,0:T(8,128)(2,1)}, u32[]{:S(2)}) copy-start(bf16[512,2048]{1,0:T(8,128)(2,1)} %all-gather.4.cloned.1.call-done) | copy-start | bytes 6291460
  86.0 49.9 %copy-start.6 = (f32[128]{0:T(128)S(1)}, f32[128]{0:T(128)}, u32[]{:S(2)}) copy-start(f32[128]{0:T(128)} %param.22) | copy-start | bytes 1540
  86.0 186.5 %all-gather.8.cloned.1.call-start = ((), (), s32[]{:S(2)}) async-start(), calls=%async_computation.3 | async-start | bytes 9437184 | tf_op jit(solution)/shard_map/all_gather | solution.py:183
  134.7 3.5 %copy-start.3 = (bf16[512,2,128]{2,0,1:T(8,128)(2,1)S(1)}, bf16[512,2,128]{2,0,1:T(8,128)(2,1)}, u32[]{:S(2)}) copy-start(bf16[512,2,128]{2,0,1:T(8,128)(2,1)} %all_gather.17) | copy-start | bytes 786436
  272.5 5.1 %copy-start.2 = (bf16[64,2048]{1,0:T(8,128)(2,1)S(1)}, bf16[64,2048]{1,0:T(8,128)(2,1)}, u32[]{:S(2)}) copy-start(bf16[64,2048]{1,0:T(8,128)(2,1)} %param.13) | copy-start | bytes 786436
Sparse Core Ops, SparseCore 0:
  56.5 23.0 all-gather.3
  86.1 99.8 all-gather.5
  187.9 54.6 all-gather.7
where the time goes:
time: 286 us; the launch traced here: 285 us
  blocking collectives  100 us (35%)
  waiting for transfers between devices  70.3 us (25%)
  matrix products  57.2 us (20%)
  other arithmetic  22.9 us (8%)
  local copies, waits for them, and re-layouts  20.4 us (7%)
  between operations  13.4 us (5%)
    all_gather x1, waiting for transfers between devices, side_by_side(): filled, at, done = (lax.all_gather(both, axis, axis=dim, tiled=True), 0, [])  46.4 us
    all_gather x1, blocking collectives, side_by_side(): filled, at, done = (lax.all_gather(both, axis, axis=dim, tiled=True), 0, [])  40.4 us
    psum x2, blocking collectives, over_axes(): value = lax.psum(value, axis)  26.1 us
    all_gather x1, waiting for transfers between devices, body(): piece = lax.all_gather(normalised_rows, 'tp', axis=0, tiled=True)  23.1 us
    dot_general x8, matrix products, update(): jnp.einsum('hqk,khd->hqd', weights_now.astype(jnp.bfloat16), value_block,...  22.2 us
    all_gather x1, blocking collectives, body(): modulation = lax.all_gather(summed, 'tp', axis=1, tiled=True)  19.5 us
    dot_general x8, matrix products, update(): jnp.einsum('hqd,khd->hqk', grouped, key_block, preferred_element_type=jnp...  18.4 us
    all_to_all x1, blocking collectives, body(): lax.all_to_all(attended, 'tp', split_axis=0, concat_axis=1, tiled=True)  14.5 us
  transfers between devices with their start and end apart: 3, of which 2 were waited for; matrix products, arithmetic and copies ran while one was open for 29% of the time, Pallas kernels for 0%

commit v1 on v0

--- a/solution.py
+++ b/solution.py
@@ -14,7 +14,11 @@
 
 def over_axes(value, axes):
     for axis in axes:
-        value = lax.psum(value, axis)
+
+        def apply_gates(base_x):
+            return jnp.sum(lax.all_gather(base_x, axis), axis=0)
+
+        value = apply_gates(value)
     return value
 
 

time: 286 us -> 299 us (1.045)
  blocking collectives: 100 us -> 110 us
    all_gather x0 -> x2, blocking collectives: none -> 32.5 us  [apply_gates(): return jnp.sum(lax.all_gather(base_x, axis), axis=0)]
    psum x2 -> x0, blocking collectives: 26.1 us -> none  [over_axes(): value = lax.psum(value, axis)]
    all_gather x1, blocking collectives: 19.5 us -> 22.9 us  [body(): modulation = lax.all_gather(summed, 'tp', axis=1, tiled=True)]
  transfers between devices with their start and end apart: 3 -> 3, of which waited for: 2 -> 2; matrix products, arithmetic and copies ran while one was open for 29% -> 28% of each run, Pallas kernels for 0% -> 0%
where the time goes in v1:
time: 299 us; the launch traced here: 298 us
  blocking collectives  110 us (37%)
  waiting for transfers between devices  73 us (24%)
  matrix products  57.2 us (19%)
  other arithmetic  23 us (8%)
  local copies, waits for them, and re-layouts  20.4 us (7%)
  between operations  13.4 us (4%)
    all_gather x1, waiting for transfers between devices, side_by_side(): filled, at, done = (lax.all_gather(both, axis, axis=dim, tiled=True), 0, [])  46.4 us
    all_gather x1, blocking collectives, side_by_side(): filled, at, done = (lax.all_gather(both, axis, axis=dim, tiled=True), 0, [])  40.5 us
    all_gather x2, blocking collectives, apply_gates(): return jnp.sum(lax.all_gather(base_x, axis), axis=0)  32.5 us
    all_gather x1, waiting for transfers between devices, body(): piece = lax.all_gather(normalised_rows, 'tp', axis=0, tiled=True)  25.9 us
    all_gather x1, blocking collectives, body(): modulation = lax.all_gather(summed, 'tp', axis=1, tiled=True)  22.9 us
    dot_general x8, matrix products, update(): jnp.einsum('hqk,khd->hqd', weights_now.astype(jnp.bfloat16), value_block,...  22.2 us
    dot_general x8, matrix products, update(): jnp.einsum('hqd,khd->hqk', grouped, key_block, preferred_element_type=jnp...  18.4 us
    all_to_all x1, blocking collectives, body(): lax.all_to_all(attended, 'tp', split_axis=0, concat_axis=1, tiled=True)  14.5 us
  transfers between devices with their start and end apart: 3, of which 2 were waited for; matrix products, arithmetic and copies ran while one was open for 28% of the time, Pallas kernels for 0%

profile of v1, /device:TPU:1, one launch (start us, length us, event | category | flops | bytes accessed | tf_op | source)
XLA Modules:
  0.0 297.8 jit_solution(6302469785545887077)
XLA Ops:
  7.8 23.1 %all-gather.2 = f32[8,2,768]{2,1,0:T(2,128)S(1)} all-gather(f32[1,2,768]{2,1,0:T(2,128)S(1)} %convolution_bitcast_fusion.1), channel_id=2, replica_groups=mesh['sp_0'=8,'sp_1'=4,'tp'=8] {'sp_0'}, dimensions={0}, use_global_device_ids=true | all-gather | bytes 55296 | tf_op jit(solution)/shard_map/all_gather | solution.py:19
  30.9 9.4 %all-gather.3 = f32[4,2,768]{2,1,0:T(2,128)S(1)} all-gather(f32[1,2,768]{2,1,0:T(2,128)S(1)} %bitcast.130), channel_id=3, replica_groups=mesh['sp_0'=8,'sp_1'=4,'tp'=8] {'sp_1'}, dimensions={0}, use_global_device_ids=true | all-gather | bytes 30720 | tf_op jit(solution)/shard_map/all_gather | solution.py:19
  40.4 22.9 %all_gather.31 = f32[2,6144]{1,0:T(2,128)S(1)} all-gather(f32[2,768]{1,0:T(2,128)S(1)} %reduce_sum.95), channel_id=1, replica_groups=mesh['sp_0'=8,'sp_1'=4,'tp'=8] {'tp'}, dimensions={1}, use_global_device_ids=true | all-gather | bytes 55296 | tf_op jit(solution)/shard_map/all_gather | solution.py:92
  66.4 25.9 %all-gather.8.cloned.1.call-done = bf16[512,2048]{1,0:T(8,128)(2,1)} async-done(((bf16[64,2048]{1,0:T(8,128)(2,1)}), bf16[512,2048]{1,0:T(8,128)(2,1)}) %all-gather.8.cloned.1.call-update) | async-done | bytes 2097168 | tf_op jit(solution)/shard_map/all_gather | solution.py:98
  92.3 2.5 multiply_reduce_fusion.3
  95.5 2.5 fusion.22
  99.5 3.0 multiply_cosine_fusion.1
  105.4 40.5 %all_gather.33 = bf16[512,2,128]{2,0,1:T(8,128)(2,1)} all-gather(bf16[16,2,128]{2,0,1:T(8,128)(2,1)S(1)} %pad_maximum_fusion.2), channel_id=1, replica_groups=mesh['sp_0'=8,'sp_1'=4,'tp'=8] {'sp_0','sp_1'}, dimensions={0}, use_global_device_ids=true | all-gather | bytes 270336 | tf_op jit(solution)/shard_map/all_gather | solution.py:27
  152.4 46.4 %all-gather.10.cloned.1.call-done = bf16[16384,2,128]{0,2,1:T(8,128)(2,1)} async-done(((bf16[512,2,128]{0,2,1:T(8,128)(2,1)}), bf16[16384,2,128]{0,2,1:T(8,128)(2,1)}) %all-gather.10.cloned.1.call-update) | async-done | bytes 8388624 | tf_op jit(solution)/shard_map/all_gather | solution.py:27
  198.8 5.8 %fusion.75 = (bf16[16384,1,128]{0,2,1:T(8,128)(2,1)}, bf16[16384,1,128]{0,2,1:T(8,128)(2,1)}) fusion(bf16[16384,2,128]{0,2,1:T(8,128)(2,1)} %all-gather.10.cloned.1.call-done), kind=kLoop, calls=%fused_computation.126 | loop fusion | bytes 16777216 | tf_op jit(solution)/shard_map/slice | solution.py:29
  204.6 6.3 %copy.29 = bf16[16384,1,128]{2,0,1:T(8,128)(2,1)} copy(bf16[16384,1,128]{0,2,1:T(8,128)(2,1)} %get-tuple-element.85) | data formatting | bytes 8388608 | tf_op jit(solution)/shard_map/while | solution.py:176
  211.0 6.5 %copy.30 = bf16[16384,1,128]{2,0,1:T(8,128)(2,1)} copy(bf16[16384,1,128]{0,2,1:T(8,128)(2,1)} %get-tuple-element.84) | data formatting | bytes 8388608 | tf_op jit(solution)/shard_map/while | solution.py:176
  217.4 52.6 %while.14 = (s32[]{:T(128)}, f32[1,1024]{1,0:T(1,128)S(1)}, f32[1,1024]{1,0:T(1,128)S(1)}, f32[1,1024,128]{2,1,0:T(8,128)S(1)}, bf16[8,2048,1,128]{3,1,2,0:T(8,1...) while((s32[]{:T(128)}, f32[1,1024]{1,0:T(1,128)S(1)}, ...), condition=%wide.region_12.13_spmd, body=%wide.region_9.12_spmd.sunk | while | flops 1090783232 | bytes 27590756 | solution.py:176
  217.4 2.3 multiply_reduce_fusion.6
  221.2 2.8 fusion.96
  227.8 2.8 fusion.96
  234.4 2.8 fusion.96
  241.0 2.8 fusion.96
  247.5 2.8 fusion.96
  254.1 2.8 fusion.96
  260.7 2.8 fusion.96
  267.2 2.8 fusion.96
  270.7 14.5 %all_to_all.19 = bf16[8,64,256]{2,1,0:T(8,128)(2,1)S(1)} all-to-all(bf16[8,64,256]{2,1,0:T(8,128)(2,1)S(1)} %all_to_all.14), channel_id=1, replica_groups=mesh['sp_0'=8,'sp_1'=4,'tp'=8] {'tp'}, dimensions={0} | all-to-all | bytes 524288 | tf_op jit(solution)/shard_map/all_to_all | solution.py:184
  285.3 5.1 %multiply_reduce_fusion.1 = (f32[64]{0:T(128)S(1)}, f32[64,2048]{1,0:T(8,128)S(1)}) fusion(bf16[64,2048]{1,0:T(8,128)(2,1)S(1)} %bitcast.113, bf16[2048,2048]{1,0:T(8,128)(2,1)} %all-gather.12.cloned.1.call-done), kind=kOutput, calls=%fused_computation.40 | convolution fusion | flops 537132992 | bytes 9175296 | tf_op jit(solution)/shard_map/dot_general | solution.py:185
  (95 shorter events, 45.2 us)
Async XLA Ops:
  6.5 139.3 %copy-start = (bf16[2048,256]{1,0:T(8,128)(2,1)S(1)}, bf16[2048,256]{1,0:T(8,128)(2,1)}, u32[]{:S(2)}) copy-start(bf16[2048,256]{1,0:T(8,128)(2,1)} %param.18) | copy-start | bytes 3145732
  6.5 88.3 %copy-start.5 = (f32[128]{0:T(128)S(1)}, f32[128]{0:T(128)}, u32[]{:S(2)}) copy-start(f32[128]{0:T(128)} %param.23) | copy-start | bytes 1540
  6.5 85.7 %all-gather.8.cloned.1.call-start = ((), (), s32[]{:S(2)}) async-start(), calls=%async_computation.1 | async-start | bytes 2359296 | tf_op jit(solution)/shard_map/all_gather | solution.py:98
  66.3 132.5 %all-gather.10.cloned.1.call-start = ((), (), s32[]{:S(2)}) async-start(), calls=%async_computation.2 | async-start | bytes 8650752 | tf_op jit(solution)/shard_map/all_gather | solution.py:27
  66.4 36.1 %copy-start.4 = (bf16[16,2048]{1,0:T(8,128)(2,1)S(1)}, bf16[16,2048]{1,0:T(8,128)(2,1)}, u32[]{:S(2)}) copy-start(bf16[16,2048]{1,0:T(8,128)(2,1)} %param.14) | copy-start | bytes 196612
  94.8 51.1 %copy-start.1 = (bf16[512,2048]{1,0:T(8,128)(2,1)S(1)}, bf16[512,2048]{1,0:T(8,128)(2,1)}, u32[]{:S(2)}) copy-start(bf16[512,2048]{1,0:T(8,128)(2,1)} %all-gather.8.cloned.1.call-done) | copy-start | bytes 6291460
  98.8 50.0 %copy-start.6 = (f32[128]{0:T(128)S(1)}, f32[128]{0:T(128)}, u32[]{:S(2)}) copy-start(f32[128]{0:T(128)} %param.22) | copy-start | bytes 1540
  98.8 186.5 %all-gather.12.cloned.1.call-start = ((), (), s32[]{:S(2)}) async-start(), calls=%async_computation.3 | async-start | bytes 9437184 | tf_op jit(solution)/shard_map/all_gather | solution.py:187
  147.4 3.5 %copy-start.3 = (bf16[512,2,128]{2,0,1:T(8,128)(2,1)S(1)}, bf16[512,2,128]{2,0,1:T(8,128)(2,1)}, u32[]{:S(2)}) copy-start(bf16[512,2,128]{2,0,1:T(8,128)(2,1)} %all_gather.33) | copy-start | bytes 786436
  285.2 5.1 %copy-start.2 = (bf16[64,2048]{1,0:T(8,128)(2,1)S(1)}, bf16[64,2048]{1,0:T(8,128)(2,1)}, u32[]{:S(2)}) copy-start(bf16[64,2048]{1,0:T(8,128)(2,1)} %param.13) | copy-start | bytes 786436
Sparse Core Ops, SparseCore 0:
  66.4 25.8 all-gather.7
  98.9 99.8 all-gather.9
  200.7 54.6 all-gather.11
